TPU v7x, 32 devices: a whole 2x2x4 slice. The times are simulated.
32 devices in a mesh: fs: 8 (over z, y), tp: 4 (over x, core).
Axes of the slice: x: 2, y: 2, z: 4, core: 2. Of those that a mesh axis runs over, the one named last changes fastest.
Arguments:
- tokens: bfloat16 [8192, 2048], P('fs', 'tp'), may hold values from -6 to 6
- mixer_gain: float32 [2048], replicated, may hold values from 0.1 to 1.9
- conv_taps: bfloat16 [3, 1024], replicated, may hold values from -3.5 to 3.5
- outer_weight: bfloat16 [2048, 1024], P('fs', 'tp'), may hold values from -0.125 to 0.125
- inner_weight: bfloat16 [2048, 1024], P('fs', 'tp'), may hold values from -0.125 to 0.125
- value_weight: bfloat16 [2048, 1024], P('fs', 'tp'), may hold values from -0.125 to 0.125
- merge_weight: bfloat16 [1024, 2048], P('tp', 'fs'), may hold values from -0.25 to 0.25
- merge_gain: float32 [2048], replicated, may hold values from 0.1 to 1.9
- channel_gain: float32 [2048], replicated, may hold values from 0.1 to 1.9
- gate_weight: bfloat16 [2048, 5632], P('fs', 'tp'), may hold values from -0.125 to 0.125
- up_weight: bfloat16 [2048, 5632], P('fs', 'tp'), may hold values from -0.125 to 0.125
- down_weight: bfloat16 [5632, 2048], P('tp', 'fs'), may hold values from -0.109375 to 0.109375
- output_gain: float32 [2048], replicated, may hold values from 0.1 to 1.9
Outputs:
- layer_out: bfloat16 [8192, 2048], P('fs', 'tp')
All inputs are finite; a program needn't handle non-finite values.
Results may differ from a plain program's by a relative error of at most 0.018.
Values may be sent and summed in bfloat16 or wider, within the bound.
A program may use at most 128 MiB of HBM per device.

v0:
```python
import jax
import jax.numpy as jnp
from jax import lax
from jax.sharding import PartitionSpec as P

HEAD_DIM = 128
EPS = 1e-06


def normalize(values):
    floats = values.astype(jnp.float32)
    return floats * lax.rsqrt(jnp.mean(floats * floats, axis=-1, keepdims=True) + EPS)


def rounded_term(partial_value):
    return lax.optimization_barrier(partial_value.astype(jnp.bfloat16)).astype(jnp.float32)


def finish_scatter(summed, residual, gain_row, squares):
    floats = summed.astype(jnp.float32)
    columns = floats.shape[1]
    factor = lax.rsqrt(squares / (columns * lax.axis_size("tp")) + EPS)
    own_gain = lax.dynamic_slice_in_dim(gain_row, lax.axis_index("tp") * columns, columns)
    return (residual.astype(jnp.float32) + floats * factor[:, None] * own_gain).astype(jnp.bfloat16)


def shards(
    tokens,
    mixer_gain,
    conv_taps,
    outer_weight,
    inner_weight,
    value_weight,
    merge_weight,
    merge_gain,
    channel_gain,
    gate_weight,
    up_weight,
    down_weight,
    output_gain,
):
    whole_tokens = lax.all_gather(tokens, "tp", axis=1, tiled=True)
    normed = (normalize(whole_tokens) * mixer_gain).astype(jnp.bfloat16)
    length = normed.shape[0]
    channels = outer_weight.shape[1]
    full_outer, full_inner, full_value = (
        lax.all_gather(outer_weight, "fs", axis=0, tiled=True),
        lax.all_gather(inner_weight, "fs", axis=0, tiled=True),
        lax.all_gather(value_weight, "fs", axis=0, tiled=True),
    )
    outer = jnp.dot(normed, full_outer, preferred_element_type=jnp.float32)
    inner = jnp.dot(normed, full_inner, preferred_element_type=jnp.float32)
    value = jnp.dot(normed, full_value, preferred_element_type=jnp.float32)
    own_taps = lax.dynamic_slice_in_dim(
        conv_taps, lax.axis_index("tp") * channels, channels, 1
    ).astype(jnp.float32)
    signal = inner * value
    padded = jnp.pad(signal, ((2, 0), (0, 0)))
    conv = (
        own_taps[0] * padded[:length]
        + own_taps[1] * padded[1 : length + 1]
        + own_taps[2] * padded[2:]
    )
    gated = (outer * conv).reshape(length, channels // HEAD_DIM, HEAD_DIM)
    mixed = normalize(gated).reshape(length, channels).astype(jnp.bfloat16)
    merged_part = jnp.dot(
        mixed,
        lax.all_gather(merge_weight, "fs", axis=1, tiled=True),
        preferred_element_type=jnp.float32,
    )
    merged = lax.psum(rounded_term(merged_part).astype(jnp.bfloat16), "tp")
    first_full = (whole_tokens.astype(jnp.float32) + normalize(merged) * merge_gain).astype(
        jnp.bfloat16
    )
    width = tokens.shape[1]
    first = lax.dynamic_slice_in_dim(first_full, lax.axis_index("tp") * width, width, 1)
    normed2 = (normalize(first_full) * channel_gain).astype(jnp.bfloat16)
    full_gate, full_up = (
        lax.all_gather(gate_weight, "fs", axis=0, tiled=True),
        lax.all_gather(up_weight, "fs", axis=0, tiled=True),
    )
    gate = jnp.dot(normed2, full_gate, preferred_element_type=jnp.float32)
    upward = jnp.dot(normed2, full_up, preferred_element_type=jnp.float32)
    hidden = (jax.nn.silu(gate) * upward).astype(jnp.bfloat16)
    down_part = jnp.dot(
        hidden,
        lax.all_gather(down_weight, "fs", axis=1, tiled=True),
        preferred_element_type=jnp.float32,
    )
    down = lax.psum_scatter(
        rounded_term(down_part).astype(jnp.bfloat16), "tp", scatter_dimension=1, tiled=True
    )
    down_float = down.astype(jnp.float32)
    down_squares = lax.psum(jnp.sum(down_float * down_float, axis=1), "tp")
    return finish_scatter(down, first, output_gain, down_squares)


def solution(mesh):
    return jax.shard_map(
        shards,
        mesh=mesh,
        in_specs=(
            P("fs", "tp"),
            P(),
            P(),
            P("fs", "tp"),
            P("fs", "tp"),
            P("fs", "tp"),
            P("tp", "fs"),
            P(),
            P(),
            P("fs", "tp"),
            P("fs", "tp"),
            P("tp", "fs"),
            P(),
        ),
        out_specs=P("fs", "tp"),
        check_vma=False,
    )
```

profile of v0, /device:TPU:0, one launch (start us, length us, event | category | flops | bytes accessed | tf_op | source)
XLA Modules:
  0.0 661.4 jit_solution(1043669761443059637)
XLA Ops:
  6.5 0.7 all-gather.9.cloned.1.call-update
  7.3 0.7 all-gather.13.cloned.1.call-update
  8.1 0.7 all-gather.15.cloned.1.call-update
  8.8 0.5 all-gather.11.cloned.1.call-update
  9.4 0.5 all-gather.17.cloned.1.call-update
  10.0 0.7 dynamic-slice_convert_fusion
  10.7 35.5 %all-gather.9.cloned.1.call-done = bf16[1024,2048]{1,0:T(8,128)(2,1)} async-done(((bf16[1024,512]{1,0:T(8,128)(2,1)}), bf16[1024,2048]{1,0:T(8,128)(2,1)}) %all-gather.9.cloned.1.call-update) | async-done | bytes 4194320 | tf_op jit(solution)/shard_map/all_gather | solution.py:42
  46.1 3.1 fusion.5
  49.2 39.4 %all-gather.13.cloned.1.call-done = bf16[2048,256]{1,0:T(8,128)(2,1)} async-done(((bf16[256,256]{1,0:T(8,128)(2,1)}), bf16[2048,256]{1,0:T(8,128)(2,1)}) %all-gather.13.cloned.1.call-update) | async-done | bytes 1048592 | tf_op jit(solution)/shard_map/all_gather | solution.py:48
  88.5 4.0 fusion.22
  92.5 37.2 %all-gather.15.cloned.1.call-done = bf16[2048,256]{1,0:T(8,128)(2,1)} async-done(((bf16[256,256]{1,0:T(8,128)(2,1)}), bf16[2048,256]{1,0:T(8,128)(2,1)}) %all-gather.15.cloned.1.call-update) | async-done | bytes 1048592 | tf_op jit(solution)/shard_map/all_gather | solution.py:49
  129.7 4.0 convolution_multiply_fusion
  133.7 37.0 %all-gather.11.cloned.1.call-done = bf16[2048,256]{1,0:T(8,128)(2,1)} async-done(((bf16[256,256]{1,0:T(8,128)(2,1)}), bf16[2048,256]{1,0:T(8,128)(2,1)}) %all-gather.11.cloned.1.call-update) | async-done | bytes 1048592 | tf_op jit(solution)/shard_map/all_gather | solution.py:47
  170.7 4.4 bitcast_reduce_fusion
  175.2 35.5 %all-gather.17.cloned.1.call-done = bf16[256,2048]{1,0:T(8,128)(2,1)} async-done(((bf16[256,256]{1,0:T(8,128)(2,1)}), bf16[256,2048]{1,0:T(8,128)(2,1)}) %all-gather.17.cloned.1.call-update) | async-done | bytes 1048592 | tf_op jit(solution)/shard_map/all_gather | solution.py:68
  210.7 4.6 convolution_convert_fusion.1
  215.4 0.7 all-gather.19.cloned.1.call-update
  216.1 0.7 all-gather.21.cloned.1.call-update
  216.9 0.7 all-gather.23.cloned.1.call-update
  217.8 82.2 %all-reduce.3.cloned.1.call-done = bf16[1024,2048]{1,0:T(8,128)(2,1)} async-done(((bf16[1024,2048]{1,0:T(8,128)(2,1)}), bf16[1024,2048]{1,0:T(8,128)(2,1)}) %all-reduce.3.cloned.1.call-update) | async-done | bytes 4194320 | tf_op jit(solution)/shard_map/psum | solution.py:71
  300.0 3.2 fusion
  303.4 5.3 fusion.2
  308.8 85.9 %all-gather.19.cloned.1.call-done = bf16[2048,1408]{1,0:T(8,128)(2,1)} async-done(((bf16[256,1408]{1,0:T(8,128)(2,1)}), bf16[2048,1408]{1,0:T(8,128)(2,1)}) %all-gather.19.cloned.1.call-update) | async-done | bytes 5767184 | tf_op jit(solution)/shard_map/all_gather | solution.py:79
  394.6 12.0 %fusion.14 = f32[1024,1408]{1,0:T(8,128)} fusion(bf16[2048,1408]{1,0:T(8,128)(2,1)} %all-gather.19.cloned.1.call-done, bf16[1024,2048]{1,0:T(8,128)(2,1)} %get-tuple-element.6, f32[2048]{0:T(1024)S(1)} %copy-done.3, f32[1024]{0:T(1024)S(1)} %add_rsqrt_fusion.2), kind=kOutput, calls=%fused_computation.27 | convolution fusion | flops 5913968640 | bytes 15740928 | tf_op jit(solution)/shard_map/dot_general | solution.py:82
  406.6 80.7 %all-gather.21.cloned.1.call-done = bf16[2048,1408]{1,0:T(8,128)(2,1)} async-done(((bf16[256,1408]{1,0:T(8,128)(2,1)}), bf16[2048,1408]{1,0:T(8,128)(2,1)}) %all-gather.21.cloned.1.call-update) | async-done | bytes 5767184 | tf_op jit(solution)/shard_map/all_gather | solution.py:80
  487.3 93.4 %all-gather.23.cloned.1.call-done = bf16[1408,2048]{1,0:T(8,128)(2,1)} async-done(((bf16[1408,256]{1,0:T(8,128)(2,1)}), bf16[1408,2048]{1,0:T(8,128)(2,1)}) %all-gather.23.cloned.1.call-update) | async-done | bytes 5767184 | tf_op jit(solution)/shard_map/all_gather | solution.py:87
  580.7 20.8 %convolution_convert_fusion = bf16[1024,2048]{1,0:T(8,128)(2,1)} fusion(bf16[1408,2048]{1,0:T(8,128)(2,1)} %all-gather.23.cloned.1.call-done, f32[1024,1408]{1,0:T(8,128)} %fusion.14, bf16[2048,1408]{1,0:T(8,128)(2,1)} %all-gather.21.cloned.1.call-done, bf16[1024,2048]{1,0:T(8,128)(2,1)} %get-tuple-element.6, f32[2048]{0:T(1024)S(1)} %copy-done.3, ...), kind=kOutput, calls=%fused_computation.17 | convolution fusion | flops 11830296576 | bytes 25702400 | tf_op jit(solution)/shard_map/dot_general | solution.py:85
  601.6 0.8 dynamic_slice.11
  602.3 42.0 %reduce-scatter.2.cloned.1.call-done = bf16[1024,512]{1,0:T(8,128)(2,1)} async-done(((bf16[1024,2048]{1,0:T(8,128)(2,1)}), bf16[1024,512]{1,0:T(8,128)(2,1)}) %reduce-scatter.2.cloned.1.call-update) | async-done | bytes 1048592 | tf_op jit(solution)/shard_map/reduce_scatter | solution.py:90
  644.3 1.5 fusion.9
  645.8 5.8 psum.15
  651.6 3.0 fusion.12
  (27 shorter events, 0.9 us)
Async XLA Ops:
  6.5 82.0 %copy-start.2 = (f32[2048]{0:T(1024)S(1)}, f32[2048]{0:T(1024)}, u32[]{:S(2)}) copy-start(f32[2048]{0:T(1024)} %param.14) | copy-start | bytes 24580
  6.5 39.6 %all-gather.9.cloned.1.call-start = ((), (), s32[]{:S(2)}) async-start(), calls=%async_computation.1 | async-start | bytes 5242880 | tf_op jit(solution)/shard_map/all_gather | solution.py:42
  7.3 81.3 %all-gather.13.cloned.1.call-start = ((), (), s32[]{:S(2)}) async-start(), calls=%async_computation.3 | async-start | bytes 1179648 | tf_op jit(solution)/shard_map/all_gather | solution.py:48
  8.0 121.7 %all-gather.15.cloned.1.call-start = ((), (), s32[]{:S(2)}) async-start(), calls=%async_computation.4 | async-start | bytes 1179648 | tf_op jit(solution)/shard_map/all_gather | solution.py:49
  8.7 162.0 %all-gather.11.cloned.1.call-start = ((), (), s32[]{:S(2)}) async-start(), calls=%async_computation.2 | async-start | bytes 1179648 | tf_op jit(solution)/shard_map/all_gather | solution.py:47
  9.3 201.4 %all-gather.17.cloned.1.call-start = ((), (), s32[]{:S(2)}) async-start(), calls=%async_computation.5 | async-start | bytes 1179648 | tf_op jit(solution)/shard_map/all_gather | solution.py:68
  9.9 290.1 %all-reduce.3.cloned.1.call-start = ((), (), s32[]{:S(2)}) async-start(), calls=%async_computation.6 | async-start | bytes 8388608 | tf_op jit(solution)/shard_map/psum | solution.py:71
  215.3 87.9 %copy-start.1 = (f32[2048]{0:T(1024)S(1)}, f32[2048]{0:T(1024)}, u32[]{:S(2)}) copy-start(f32[2048]{0:T(1024)} %param.20) | copy-start | bytes 24580
  215.3 179.3 %all-gather.19.cloned.1.call-start = ((), (), s32[]{:S(2)}) async-start(), calls=%async_computation.7 | async-start | bytes 6488064 | tf_op jit(solution)/shard_map/all_gather | solution.py:79
  216.1 271.3 %all-gather.21.cloned.1.call-start = ((), (), s32[]{:S(2)}) async-start(), calls=%async_computation.8 | async-start | bytes 6488064 | tf_op jit(solution)/shard_map/all_gather | solution.py:80
  216.8 363.9 %all-gather.23.cloned.1.call-start = ((), (), s32[]{:S(2)}) async-start(), calls=%async_computation.9 | async-start | bytes 6488064 | tf_op jit(solution)/shard_map/all_gather | solution.py:87
  217.5 426.8 %reduce-scatter.2.cloned.1.call-start = ((), (), s32[]{:S(2)}) async-start(), calls=%async_computation.10 | async-start | bytes 5242880 | tf_op jit(solution)/shard_map/reduce_scatter | solution.py:90
  300.0 3.4 copy-start
  303.4 91.2 %copy-start.3 = (f32[2048]{0:T(1024)S(1)}, f32[2048]{0:T(1024)}, u32[]{:S(2)}) copy-start(f32[2048]{0:T(1024)} %param.21) | copy-start | bytes 24580
Sparse Core Ops, SparseCore 0:
  8.9 37.1 all-gather.8
  48.2 40.2 all-gather.12
  90.7 38.9 all-gather.14
  131.7 38.9 all-gather.10
  172.6 38.0 all-gather.16
  215.4 84.4 all-reduce.2
  302.1 92.4 all-gather.18
  396.8 90.4 all-gather.20
  489.4 91.2 all-gather.22
  601.7 42.5 reduce-scatter.1
where the time goes:
time: 662 us; the launch traced here: 661 us
  waiting for transfers between devices  574 us (87%)
  matrix products  49.7 us (8%)
  other arithmetic  16.9 us (3%)
  between operations  13.6 us (2%)
    all_gather x1, waiting for transfers between devices, shards(): lax.all_gather(down_weight, 'fs', axis=1, tiled=True)  93.4 us
    all_gather x1, waiting for transfers between devices, shards(): lax.all_gather(gate_weight, 'fs', axis=0, tiled=True)  85.9 us
    psum x1, waiting for transfers between devices, shards(): merged = lax.psum(rounded_term(merged_part).astype(jnp.bfloat16), 'tp')  82.2 us
    all_gather x1, waiting for transfers between devices, shards(): lax.all_gather(up_weight, 'fs', axis=0, tiled=True)  80.7 us
    reduce_scatter x1, waiting for transfers between devices, shards(): lax.psum_scatter(rounded_term(down_part).astype(jnp.bfloat16), 'tp', scat...  42 us
    all_gather x1, waiting for transfers between devices, shards(): lax.all_gather(inner_weight, 'fs', axis=0, tiled=True)  39.4 us
    all_gather x1, waiting for transfers between devices, shards(): lax.all_gather(value_weight, 'fs', axis=0, tiled=True)  37.2 us
    all_gather x1, waiting for transfers between devices, shards(): lax.all_gather(outer_weight, 'fs', axis=0, tiled=True)  37 us
  transfers between devices with their start and end apart: 10, of which 10 were waited for; matrix products, arithmetic and copies ran while one was open for 6% of the time, Pallas kernels for 0%

commit v1 on v0

--- a/solution.py
+++ b/solution.py
@@ -68,7 +68,9 @@
         lax.all_gather(merge_weight, "fs", axis=1, tiled=True),
         preferred_element_type=jnp.float32,
     )
-    merged = lax.psum(rounded_term(merged_part).astype(jnp.bfloat16), "tp")
+    part = rounded_term(merged_part).astype(jnp.bfloat16)
+    blocks = lax.all_gather(part, "tp", axis=0, tiled=False)
+    merged = blocks.sum(axis=0)
     first_full = (whole_tokens.astype(jnp.float32) + normalize(merged) * merge_gain).astype(
         jnp.bfloat16
     )

time: 662 us -> 682 us (1.030)
  other arithmetic: 16.9 us -> 29.2 us
  waiting for transfers between devices: 574 us -> 582 us
    all_gather x0 -> x1, waiting for transfers between devices: none -> 103 us  [shards(): blocks = lax.all_gather(part, 'tp', axis=0, tiled=False)]
    psum x1 -> x0, waiting for transfers between devices: 82.2 us -> none  [shards(): merged = lax.psum(rounded_term(merged_part).astype(jnp.bfloat16), 'tp')]
    all_gather x1, waiting for transfers between devices: 85.9 us -> 73.5 us  [shards(): lax.all_gather(gate_weight, 'fs', axis=0, tiled=True)]
    reduce_sum x0 -> x1, other arithmetic: none -> 12.1 us  [shards(): merged = blocks.sum(axis=0)]
  transfers between devices with their start and end apart: 10 -> 10, of which waited for: 10 -> 10; matrix products, arithmetic and copies ran while one was open for 6% -> 7% of each run, Pallas kernels for 0% -> 0%
where the time goes in v1:
time: 682 us
  waiting for transfers between devices  582 us (85%)
  matrix products  49.7 us (7%)
  other arithmetic  29.2 us (4%)
  between operations  13.6 us (2%)
    all_gather x1, waiting for transfers between devices, shards(): blocks = lax.all_gather(part, 'tp', axis=0, tiled=False)  103 us
    all_gather x1, waiting for transfers between devices, shards(): lax.all_gather(down_weight, 'fs', axis=1, tiled=True)  93.4 us
    all_gather x1, waiting for transfers between devices, shards(): lax.all_gather(up_weight, 'fs', axis=0, tiled=True)  80.8 us
    all_gather x1, waiting for transfers between devices, shards(): lax.all_gather(gate_weight, 'fs', axis=0, tiled=True)  73.5 us
    reduce_scatter x1, waiting for transfers between devices, shards(): lax.psum_scatter(rounded_term(down_part).astype(jnp.bfloat16), 'tp', scat...  42 us
    all_gather x1, waiting for transfers between devices, shards(): lax.all_gather(inner_weight, 'fs', axis=0, tiled=True)  39.4 us
    all_gather x1, waiting for transfers between devices, shards(): lax.all_gather(value_weight, 'fs', axis=0, tiled=True)  37.2 us
    all_gather x1, waiting for transfers between devices, shards(): lax.all_gather(outer_weight, 'fs', axis=0, tiled=True)  37 us
  transfers between devices with their start and end apart: 10, of which 10 were waited for; matrix products, arithmetic and copies ran while one was open for 7% of the time, Pallas kernels for 0%

profile of v1, /device:TPU:0, one launch (start us, length us, event | category | flops | bytes accessed | tf_op | source)
XLA Modules:
  0.0 681.7 jit_solution(1234677315943103706)
XLA Ops:
  6.5 0.7 all-gather.11.cloned.1.call-update
  7.3 0.7 all-gather.15.cloned.1.call-update
  8.1 0.7 all-gather.17.cloned.1.call-update
  9.4 0.5 all-gather.19.cloned.1.call-update
  10.0 0.7 dynamic-slice_convert_fusion
  10.7 35.5 %all-gather.11.cloned.1.call-done = bf16[1024,2048]{1,0:T(8,128)(2,1)} async-done(((bf16[1024,512]{1,0:T(8,128)(2,1)}), bf16[1024,2048]{1,0:T(8,128)(2,1)}) %all-gather.11.cloned.1.call-update) | async-done | bytes 4194320 | tf_op jit(solution)/shard_map/all_gather | solution.py:42
  46.1 3.1 fusion.5
  49.2 39.4 %all-gather.15.cloned.1.call-done = bf16[2048,256]{1,0:T(8,128)(2,1)} async-done(((bf16[256,256]{1,0:T(8,128)(2,1)}), bf16[2048,256]{1,0:T(8,128)(2,1)}) %all-gather.15.cloned.1.call-update) | async-done | bytes 1048592 | tf_op jit(solution)/shard_map/all_gather | solution.py:48
  88.5 4.0 fusion.22
  92.5 37.2 %all-gather.17.cloned.1.call-done = bf16[2048,256]{1,0:T(8,128)(2,1)} async-done(((bf16[256,256]{1,0:T(8,128)(2,1)}), bf16[2048,256]{1,0:T(8,128)(2,1)}) %all-gather.17.cloned.1.call-update) | async-done | bytes 1048592 | tf_op jit(solution)/shard_map/all_gather | solution.py:49
  129.7 4.0 convolution_multiply_fusion
  133.7 37.0 %all-gather.13.cloned.1.call-done = bf16[2048,256]{1,0:T(8,128)(2,1)} async-done(((bf16[256,256]{1,0:T(8,128)(2,1)}), bf16[2048,256]{1,0:T(8,128)(2,1)}) %all-gather.13.cloned.1.call-update) | async-done | bytes 1048592 | tf_op jit(solution)/shard_map/all_gather | solution.py:47
  170.7 4.4 bitcast_reduce_fusion
  175.2 35.5 %all-gather.19.cloned.1.call-done = bf16[256,2048]{1,0:T(8,128)(2,1)} async-done(((bf16[256,256]{1,0:T(8,128)(2,1)}), bf16[256,2048]{1,0:T(8,128)(2,1)}) %all-gather.19.cloned.1.call-update) | async-done | bytes 1048592 | tf_op jit(solution)/shard_map/all_gather | solution.py:68
  210.7 4.5 convolution_convert_fusion.1
  215.3 0.7 all-gather.21.cloned.1.call-update
  216.1 0.7 all-gather.23.cloned.1.call-update
  216.8 0.7 all-gather.25.cloned.1.call-update
  217.7 102.6 %all-gather.27.cloned.1.call-done = bf16[4096,2048]{1,0:T(8,128)(2,1)} async-done(((bf16[1024,2048]{1,0:T(8,128)(2,1)}), bf16[4096,2048]{1,0:T(8,128)(2,1)}) %all-gather.27.cloned.1.call-update) | async-done | bytes 16777232 | tf_op jit(solution)/shard_map/all_gather | solution.py:72
  320.3 12.1 %reduce_sum.59 = bf16[1024,2048]{1,0:T(8,128)(2,1)} reduce(bf16[4,1024,2048]{2,1,0:T(8,128)(2,1)} %bitcast.23, bf16[]{:T(256)} %constant.32.clone.1), dimensions={0}, to_apply=%region_2.3 | reduce | flops 6291456 | bytes 20971522 | tf_op jit(solution)/shard_map/reduce_sum | solution.py:73
  332.4 3.2 fusion
  335.9 5.5 fusion.2
  341.4 73.5 %all-gather.21.cloned.1.call-done = bf16[2048,1408]{1,0:T(8,128)(2,1)} async-done(((bf16[256,1408]{1,0:T(8,128)(2,1)}), bf16[2048,1408]{1,0:T(8,128)(2,1)}) %all-gather.21.cloned.1.call-update) | async-done | bytes 5767184 | tf_op jit(solution)/shard_map/all_gather | solution.py:81
  414.9 11.9 %fusion.14 = f32[1024,1408]{1,0:T(8,128)} fusion(bf16[2048,1408]{1,0:T(8,128)(2,1)} %all-gather.21.cloned.1.call-done, bf16[1024,2048]{1,0:T(8,128)(2,1)} %get-tuple-element.6, f32[2048]{0:T(1024)S(1)} %copy-done.3, f32[1024]{0:T(1024)S(1)} %add_rsqrt_fusion.2), kind=kOutput, calls=%fused_computation.27 | convolution fusion | flops 5913968640 | bytes 15740928 | tf_op jit(solution)/shard_map/dot_general | solution.py:84
  426.8 80.8 %all-gather.23.cloned.1.call-done = bf16[2048,1408]{1,0:T(8,128)(2,1)} async-done(((bf16[256,1408]{1,0:T(8,128)(2,1)}), bf16[2048,1408]{1,0:T(8,128)(2,1)}) %all-gather.23.cloned.1.call-update) | async-done | bytes 5767184 | tf_op jit(solution)/shard_map/all_gather | solution.py:82
  507.6 93.4 %all-gather.25.cloned.1.call-done = bf16[1408,2048]{1,0:T(8,128)(2,1)} async-done(((bf16[1408,256]{1,0:T(8,128)(2,1)}), bf16[1408,2048]{1,0:T(8,128)(2,1)}) %all-gather.25.cloned.1.call-update) | async-done | bytes 5767184 | tf_op jit(solution)/shard_map/all_gather | solution.py:89
  601.0 20.9 %convolution_convert_fusion = bf16[1024,2048]{1,0:T(8,128)(2,1)} fusion(bf16[1408,2048]{1,0:T(8,128)(2,1)} %all-gather.25.cloned.1.call-done, f32[1024,1408]{1,0:T(8,128)} %fusion.14, bf16[2048,1408]{1,0:T(8,128)(2,1)} %all-gather.23.cloned.1.call-done, bf16[1024,2048]{1,0:T(8,128)(2,1)} %get-tuple-element.6, f32[2048]{0:T(1024)S(1)} %copy-done.3, ...), kind=kOutput, calls=%fused_computation.17 | convolution fusion | flops 11830296576 | bytes 25702400 | tf_op jit(solution)/shard_map/dot_general | solution.py:87
  621.9 0.8 dynamic_slice.11
  622.6 42.0 %reduce-scatter.2.cloned.1.call-done = bf16[1024,512]{1,0:T(8,128)(2,1)} async-done(((bf16[1024,2048]{1,0:T(8,128)(2,1)}), bf16[1024,512]{1,0:T(8,128)(2,1)}) %reduce-scatter.2.cloned.1.call-update) | async-done | bytes 1048592 | tf_op jit(solution)/shard_map/reduce_scatter | solution.py:92
  664.6 1.5 fusion.9
  666.1 5.8 psum.7
  671.9 3.0 fusion.12
  (28 shorter events, 1.4 us)
Async XLA Ops:
  6.5 82.0 %copy-start.2 = (f32[2048]{0:T(1024)S(1)}, f32[2048]{0:T(1024)}, u32[]{:S(2)}) copy-start(f32[2048]{0:T(1024)} %param.14) | copy-start | bytes 24580
  6.5 39.6 %all-gather.11.cloned.1.call-start = ((), (), s32[]{:S(2)}) async-start(), calls=%async_computation.1 | async-start | bytes 5242880 | tf_op jit(solution)/shard_map/all_gather | solution.py:42
  7.3 81.3 %all-gather.15.cloned.1.call-start = ((), (), s32[]{:S(2)}) async-start(), calls=%async_computation.3 | async-start | bytes 1179648 | tf_op jit(solution)/shard_map/all_gather | solution.py:48
  8.0 121.7 %all-gather.17.cloned.1.call-start = ((), (), s32[]{:S(2)}) async-start(), calls=%async_computation.4 | async-start | bytes 1179648 | tf_op jit(solution)/shard_map/all_gather | solution.py:49
  8.7 162.0 %all-gather.13.cloned.1.call-start = ((), (), s32[]{:S(2)}) async-start(), calls=%async_computation.2 | async-start | bytes 1179648 | tf_op jit(solution)/shard_map/all_gather | solution.py:47
  9.3 201.4 %all-gather.19.cloned.1.call-start = ((), (), s32[]{:S(2)}) async-start(), calls=%async_computation.5 | async-start | bytes 1179648 | tf_op jit(solution)/shard_map/all_gather | solution.py:68
  9.9 310.4 %all-gather.27.cloned.1.call-start = ((), (), s32[]{:S(2)}) async-start(), calls=%async_computation.10 | async-start | bytes 20971520 | tf_op jit(solution)/shard_map/all_gather | solution.py:72
  215.3 199.6 %all-gather.21.cloned.1.call-start = ((), (), s32[]{:S(2)}) async-start(), calls=%async_computation.6 | async-start | bytes 6488064 | tf_op jit(solution)/shard_map/all_gather | solution.py:81
  216.0 291.5 %all-gather.23.cloned.1.call-start = ((), (), s32[]{:S(2)}) async-start(), calls=%async_computation.7 | async-start | bytes 6488064 | tf_op jit(solution)/shard_map/all_gather | solution.py:82
  216.8 384.2 %all-gather.25.cloned.1.call-start = ((), (), s32[]{:S(2)}) async-start(), calls=%async_computation.8 | async-start | bytes 6488064 | tf_op jit(solution)/shard_map/all_gather | solution.py:89
  217.5 447.1 %reduce-scatter.2.cloned.1.call-start = ((), (), s32[]{:S(2)}) async-start(), calls=%async_computation.9 | async-start | bytes 5242880 | tf_op jit(solution)/shard_map/reduce_scatter | solution.py:92
  320.3 15.3 %copy-start.1 = (f32[2048]{0:T(1024)S(1)}, f32[2048]{0:T(1024)}, u32[]{:S(2)}) copy-start(f32[2048]{0:T(1024)} %param.20) | copy-start | bytes 24580
  332.4 3.4 copy-start
  335.9 79.0 %copy-start.3 = (f32[2048]{0:T(1024)S(1)}, f32[2048]{0:T(1024)}, u32[]{:S(2)}) copy-start(f32[2048]{0:T(1024)} %param.21) | copy-start | bytes 24580
Sparse Core Ops, SparseCore 0:
  8.9 37.1 all-gather.10
  48.2 40.2 all-gather.14
  90.7 38.9 all-gather.16
  131.7 38.9 all-gather.12
  172.6 38.0 all-gather.18
  215.4 104.8 all-gather.26
  322.5 92.3 all-gather.20
  417.0 90.4 all-gather.22
  509.6 91.2 all-gather.24
  622.0 42.5 reduce-scatter.1
